TPU v7x, 512 devices: a whole 4x4x16 slice. The times are simulated.
512 devices in a mesh: ep: 16 (over y, x), tp: 32 (over z, core).
Axes of the slice: x: 4, y: 4, z: 16, core: 2. Of those that a mesh axis runs over, the one named last changes fastest.
Arguments:
- tokens: bfloat16 [8192, 4096], P('tp', 'ep'), may hold values from -20 to 20
- norm_gain: bfloat16 [4096], P('ep'), may hold values from 0.099609375 to 1.8984375
- expert_ids: int32 [8192, 2], P('tp'), may hold values from 0 to 31, all different within a row; in each aligned block of 256 rows (0 to 255, 256 to 511, ...) at most 32 rows name the same one
- combine_weight: float32 [8192, 2], P('tp'), may hold values from 0.05 to 1
- w_gate: bfloat16 [32, 2048, 4096], P('tp', 'ep'), may hold values from -0.09375 to 0.09375
- w_up: bfloat16 [32, 2048, 4096], P('tp', 'ep'), may hold values from -0.09375 to 0.09375
- w_down: bfloat16 [32, 2048, 4096], P('tp', None, 'ep'), may hold values from -2 to 2
- out_gain: bfloat16 [4096], P('ep'), may hold values from 0.099609375 to 1.8984375
Outputs:
- mixed: bfloat16 [8192, 4096], P('tp', 'ep')
Inputs may be any that keep to these rules, and one draw needn't show every extreme that they name: `expert_ids`: each row names 2 different experts; among the rows of one index of tp no expert is named by more than 32 rows, a bound that some block reaches.
All inputs are finite; a program needn't handle non-finite values.
Results may differ from a plain program's by a relative error of at most 0.007.
Values may be sent and summed in bfloat16 or wider, within the bound.
No kernel may reach another device: no remote copies, remote signals or barrier semaphores. Data moves between devices by JAX's collectives and lax.ppermute only.
A program may use at most 64 MiB of HBM per device.

v0:
```python
import jax
import jax.numpy as jnp
from jax import lax
from jax.sharding import Mesh
from jax.sharding import PartitionSpec as P

TP = ("tp_0", "tp_1")
epsilon = 1e-06


def sent_to_all(value, axis):
    copies = jnp.broadcast_to(value, (lax.axis_size(axis), *value.shape))
    return lax.all_to_all(copies, axis, split_axis=0, concat_axis=0, tiled=True)


def over_copies(value, axis):
    everything = sent_to_all(value, axis)
    return jnp.sum(everything, axis=0)


def cut_along(value, dim, peers):
    before, after = (value.shape[:dim], value.shape[dim + 1 :])
    return jnp.moveaxis(value.reshape(*before, peers, -1, *after), dim, 0)


def in_order(parts, dim):
    parts = jnp.moveaxis(parts, 0, dim)
    lengths = parts.shape
    return parts.reshape(*lengths[:dim], lengths[dim] * lengths[dim + 1], *lengths[dim + 2 :])


def turned_blocks(parts, axes, turns):
    lengths = [lax.axis_size(a) for a in axes]
    parts = parts.reshape(*lengths, *parts.shape[1:])
    for k in turns:
        parts = lax.all_to_all(parts, axes[k], split_axis=k, concat_axis=k, tiled=True)
    return parts.reshape(-1, *parts.shape[len(axes) :])


def core_and_chips(value, groups, turns, split_dim, concat_dim):
    peers = lax.axis_size(groups[0]) * lax.axis_size(groups[1])
    parts = cut_along(value, split_dim, peers)
    return in_order(turned_blocks(parts, groups, turns), concat_dim)


def body(tokens, norm_gain, expert_ids, combine_weight, w_gate, w_up, w_down, out_gain):
    tok_rows, width_local = tokens.shape
    n_split = lax.axis_size("ep")
    n_route = lax.axis_size(TP)
    width = width_local * n_split
    local_experts = w_gate.shape[0]
    total_experts = local_experts * n_route
    top = expert_ids.shape[1]
    capacity = 2 * top * tok_rows // total_experts
    flat_ids = expert_ids.reshape(-1)
    onehot = (flat_ids[:, None] == jnp.arange(total_experts, dtype=jnp.int32)[None, :]).astype(
        jnp.int32
    )
    ranks = jnp.sum((jnp.cumsum(onehot, axis=0) - 1) * onehot, axis=1)
    target = flat_ids * capacity + ranks
    source_rows = jnp.arange(tok_rows * top, dtype=jnp.int32) // top
    xf = tokens.astype(jnp.float32)
    squares = over_copies(jnp.sum(xf * xf, axis=1), "ep")
    normed = (
        xf * lax.rsqrt(squares / width + epsilon)[:, None] * norm_gain.astype(jnp.float32)[None, :]
    ).astype(jnp.bfloat16)
    buffer = (
        jnp.zeros((total_experts * capacity, width_local), jnp.bfloat16)
        .at[target]
        .set(normed[source_rows])
    )
    arrived = lax.all_to_all(buffer, TP, split_axis=0, concat_axis=0, tiled=True)
    arrived = arrived.reshape(n_route, local_experts, capacity, width_local)
    piece = lax.all_gather(arrived, "ep", axis=3, tiled=True)
    gate_sum = jnp.einsum("sect,eft->secf", piece, w_gate, preferred_element_type=jnp.float32)
    up_sum = jnp.einsum("sect,eft->secf", piece, w_up, preferred_element_type=jnp.float32)
    hidden = (jax.nn.silu(gate_sum) * up_sum).astype(jnp.bfloat16)
    result = jnp.einsum(
        "secf,efd->secd",
        lax.all_gather(hidden, "ep", axis=3, tiled=True),
        w_down,
        preferred_element_type=jnp.float32,
    )
    expert_out = result.astype(jnp.bfloat16).reshape(
        n_route * local_experts * capacity, width_local
    )
    returned = core_and_chips(expert_out, ("tp_0", "tp_1"), (1, 0), 0, 0)
    picked = returned[target].astype(jnp.float32).reshape(tok_rows, top, width_local)
    moe = jnp.sum(picked * combine_weight[:, :, None], axis=1)
    squares_out = over_copies(jnp.sum(moe * moe, axis=1), "ep")
    mixed = (
        moe
        * lax.rsqrt(squares_out / width + epsilon)[:, None]
        * out_gain.astype(jnp.float32)[None, :]
    )
    return mixed.astype(jnp.bfloat16)


def solution(mesh):
    finer = Mesh(mesh.devices.reshape(mesh.shape["ep"], 16, 2), ("ep", "tp_0", "tp_1"))
    return jax.shard_map(
        body,
        mesh=finer,
        in_specs=(
            P(TP, "ep"),
            P("ep"),
            P(TP, None),
            P(TP, None),
            P(TP, "ep", None),
            P(TP, "ep", None),
            P(TP, None, "ep"),
            P("ep"),
        ),
        out_specs=P(TP, "ep"),
        check_vma=False,
    )
```

profile of v0, /device:TPU:32, one launch (start us, length us, event | category | flops | bytes accessed | tf_op | source)
XLA Modules:
  0.0 313.2 jit_solution(1302803057971697116)
XLA Ops:
  6.5 1.1 fusion.10
  7.6 0.6 broadcast_in_dim.7
  8.3 7.0 %all-to-all-start = ((f32[16,1,256]{2,1,0:T(1,128)}), f32[16,1,256]{2,1,0:T(1,128)S(1)}, u32[]{:S(2)}, u32[]{:S(2)}) async-start(f32[16,1,256]{2,1,0:T(1,128)} %broadcast_in_dim.7), calls=%async_computation | async-start | bytes 32768 | tf_op jit(solution)/shard_map/all_to_all | solution.py:13
  15.4 0.8 copy.37
  16.2 0.1 eq.29
  16.3 0.1 eq.25
  16.5 0.7 broadcast_multiply_fusion
  17.2 1.2 reduce-window.6
  18.3 0.2 slice_reduce_fusion
  18.6 0.1 copy.36
  18.8 0.1 mul.74
  19.0 0.7 convert_element_type.44
  19.7 3.2 %all-to-all-done = f32[16,1,256]{2,1,0:T(1,128)S(1)} async-done(((f32[16,1,256]{2,1,0:T(1,128)}), f32[16,1,256]{2,1,0:T(1,128)S(1)}, u32[]{:S(2)}, u32[]{:S(2)}) %all-to-all-start) | async-done | bytes 16416 | tf_op jit(solution)/shard_map/all_to_all | solution.py:13
  22.9 1.0 fusion.12
  24.0 3.9 %scatter_custom_fusion = bf16[1024,256]{1,0:T(8,128)(2,1)S(1)} fusion(s32[512]{0:T(512)S(1)} %bitcast.65, bf16[256,256]{1,0:T(8,128)(2,1)S(1)} %fusion.12, s32[1024]{0:T(1024)S(1)} %pad_clamp_fusion.1, bf16[]{:T(256)} %constant.32.clone.1), kind=kCustom, calls=%fused_computation.19 | custom fusion | bytes 524290 | tf_op jit(solution)/shard_map/scatter | solution.py:70
  27.9 47.4 %all_to_all.31 = bf16[32,32,256]{2,1,0:T(8,128)(2,1)} all-to-all(bf16[32,32,256]{2,1,0:T(8,128)(2,1)S(1)} %bitcast.63), channel_id=1, replica_groups=mesh['ep'=16,'tp_0'=16,'tp_1'=2] {'tp_0','tp_1'}, dimensions={0} | all-to-all | bytes 1048576 | tf_op jit(solution)/shard_map/all_to_all | solution.py:72
  75.4 82.4 %all-gather.6.cloned.1.call-done = bf16[32,32,4096]{2,1,0:T(8,128)(2,1)} async-done(((bf16[32,32,256]{2,1,0:T(8,128)(2,1)}), bf16[32,32,4096]{2,1,0:T(8,128)(2,1)}) %all-gather.6.cloned.1.call-update) | async-done | bytes 8388624 | tf_op jit(solution)/shard_map/all_gather | solution.py:74
  157.9 6.1 %convolution_bitcast_fusion.1 = f32[32,1,32,128]{3,2,0,1:T(8,128)S(1)} fusion(bf16[32,32,4096]{2,1,0:T(8,128)(2,1)} %all-gather.6.cloned.1.call-done, bf16[1,128,4096]{2,1,0:T(8,128)(2,1)} %param.12), kind=kOutput, calls=%fused_computation.8 | convolution fusion | flops 1073741824 | bytes 9961472 | tf_op jit(solution)/shard_map/sect,eft->secf/dot_general | solution.py:75
  164.0 3.0 fusion.6
  167.0 71.7 %all-gather.4.cloned.1.call-done = bf16[32,1,32,2048]{3,2,0,1:T(8,128)(2,1)} async-done(((bf16[32,1,32,128]{3,2,0,1:T(8,128)(2,1)}), bf16[32,1,32,2048]{3,2,0,1:T(8,128)(2,1)}) %all-gather.4.cloned.1.call-update) | async-done | bytes 4194320 | tf_op jit(solution)/shard_map/all_gather | solution.py:80
  238.8 3.4 %fusion.2 = bf16[32,32,256]{2,1,0:T(8,128)(2,1)S(1)} fusion(bf16[32,1,32,2048]{3,2,0,1:T(8,128)(2,1)} %all-gather.4.cloned.1.call-done, bf16[1,2048,256]{2,1,0:T(8,128)(2,1)S(1)} %copy-done), kind=kOutput, calls=%fused_computation.5 | convolution fusion | flops 1074003968 | bytes 5767168 | tf_op jit(solution)/shard_map/secf,efd->secd/dot_general | solution.py:78
  242.3 4.2 %all_to_all.32 = bf16[16,2,32,256]{3,2,0,1:T(8,128)(2,1)S(1)} all-to-all(bf16[16,2,32,256]{3,2,0,1:T(8,128)(2,1)S(1)} %copy.41), channel_id=1, replica_groups=mesh['ep'=16,'tp_0'=16,'tp_1'=2] {'tp_1'}, dimensions={1} | all-to-all | bytes 1048576 | tf_op jit(solution)/shard_map/all_to_all | solution.py:36
  246.4 0.8 copy.42
  247.3 12.7 %all-to-all-start.3 = ((bf16[16,2,32,256]{3,2,1,0:T(8,128)(2,1)}), bf16[16,2,32,256]{3,2,1,0:T(8,128)(2,1)S(1)}, u32[]{:S(2)}, u32[]{:S(2)}) async-start(bf16[16,2,32,256]{3,2,1,0:T(8,128)(2,1)} %copy.42), calls=%async_computation.3 | async-start | bytes 1048576 | tf_op jit(solution)/shard_map/all_to_all | solution.py:36
  260.1 29.2 %all-to-all-done.3 = bf16[16,2,32,256]{3,2,1,0:T(8,128)(2,1)S(1)} async-done(((bf16[16,2,32,256]{3,2,1,0:T(8,128)(2,1)}), bf16[16,2,32,256]{3,2,1,0:T(8,128)(2,1)S(1)}, u32[]{:S(2)}, u32[]{:S(2)}) %all-to-all-start.3) | async-done | bytes 524320 | tf_op jit(solution)/shard_map/all_to_all | solution.py:36
  289.3 1.9 gather_fusion
  291.3 0.3 reshape.149
  291.5 0.7 multiply_reduce_fusion
  292.4 0.6 broadcast_in_dim.8
  293.0 4.9 %all-to-all-start.4 = ((f32[16,1,256]{2,1,0:T(1,128)}), f32[16,1,256]{2,1,0:T(1,128)S(1)}, u32[]{:S(2)}, u32[]{:S(2)}) async-start(f32[16,1,256]{2,1,0:T(1,128)} %broadcast_in_dim.8), calls=%async_computation.4 | async-start | bytes 32768 | tf_op jit(solution)/shard_map/all_to_all | solution.py:13
  297.9 7.6 %all-to-all-done.4 = f32[16,1,256]{2,1,0:T(1,128)S(1)} async-done(((f32[16,1,256]{2,1,0:T(1,128)}), f32[16,1,256]{2,1,0:T(1,128)S(1)}, u32[]{:S(2)}, u32[]{:S(2)}) %all-to-all-start.4) | async-done | bytes 16416 | tf_op jit(solution)/shard_map/all_to_all | solution.py:13
  305.6 0.8 multiply_convert_fusion
  (30 shorter events, 0.7 us)
Async XLA Ops:
  6.5 232.2 %copy-start = (bf16[1,2048,256]{2,1,0:T(8,128)(2,1)S(1)}, bf16[1,2048,256]{2,1,0:T(8,128)(2,1)}, u32[]{:S(2)}) copy-start(bf16[1,2048,256]{2,1,0:T(8,128)(2,1)} %param.14) | copy-start | bytes 3145732
  8.3 14.6 %all-to-all-start = ((f32[16,1,256]{2,1,0:T(1,128)}), f32[16,1,256]{2,1,0:T(1,128)S(1)}, u32[]{:S(2)}, u32[]{:S(2)}) async-start(f32[16,1,256]{2,1,0:T(1,128)} %broadcast_in_dim.7), calls=%async_computation | async-start | bytes 32768 | tf_op jit(solution)/shard_map/all_to_all | solution.py:13
  15.3 142.5 %all-gather.6.cloned.1.call-start = ((), (), s32[]{:S(2)}) async-start(), calls=%async_computation.6 | async-start | bytes 8912896 | tf_op jit(solution)/shard_map/all_gather | solution.py:74
  75.3 88.6 %copy-start.3 = (bf16[1,128,4096]{2,1,0:T(8,128)(2,1)S(1)}, bf16[1,128,4096]{2,1,0:T(8,128)(2,1)}, u32[]{:S(2)}) copy-start(bf16[1,128,4096]{2,1,0:T(8,128)(2,1)} %param.13) | copy-start | bytes 3145732
  75.4 163.4 %all-gather.4.cloned.1.call-start = ((), (), s32[]{:S(2)}) async-start(), calls=%async_computation.5 | async-start | bytes 4456448 | tf_op jit(solution)/shard_map/all_gather | solution.py:80
  157.9 6.1 %copy-start.2 = (bf16[32,32,4096]{2,1,0:T(8,128)(2,1)S(1)}, bf16[32,32,4096]{2,1,0:T(8,128)(2,1)}, u32[]{:S(2)}) copy-start(bf16[32,32,4096]{2,1,0:T(8,128)(2,1)} %all-gather.6.cloned.1.call-done) | copy-start | bytes 25165828
  167.0 92.9 %copy-start.1 = (f32[256,2]{0,1:T(2,128)S(1)}, f32[256,2]{0,1:T(2,128)}, u32[]{:S(2)}) copy-start(f32[256,2]{0,1:T(2,128)} %param.11) | copy-start | bytes 6148
  167.0 130.9 %copy-start.4 = (bf16[256]{0:T(256)(128)(2,1)S(1)}, bf16[256]{0:T(256)(128)(2,1)}, u32[]{:S(2)}) copy-start(bf16[256]{0:T(256)(128)(2,1)} %param.15) | copy-start | bytes 1540
  247.3 42.1 %all-to-all-start.3 = ((bf16[16,2,32,256]{3,2,1,0:T(8,128)(2,1)}), bf16[16,2,32,256]{3,2,1,0:T(8,128)(2,1)S(1)}, u32[]{:S(2)}, u32[]{:S(2)}) async-start(bf16[16,2,32,256]{3,2,1,0:T(8,128)(2,1)} %copy.42), calls=%async_computation.3 | async-start | bytes 1048576 | tf_op jit(solution)/shard_map/all_to_all | solution.py:36
  293.0 12.5 %all-to-all-start.4 = ((f32[16,1,256]{2,1,0:T(1,128)}), f32[16,1,256]{2,1,0:T(1,128)S(1)}, u32[]{:S(2)}, u32[]{:S(2)}) async-start(f32[16,1,256]{2,1,0:T(1,128)} %broadcast_in_dim.8), calls=%async_computation.4 | async-start | bytes 32768 | tf_op jit(solution)/shard_map/all_to_all | solution.py:13
Sparse Core Ops, SparseCore 0:
  75.5 82.3 all-gather.5
  167.2 71.5 all-gather.3
where the time goes:
time: 314 us; the launch traced here: 313 us
  waiting for transfers between devices  194 us (62%)
  blocking collectives  51.6 us (16%)
  starting transfers between devices  24.7 us (8%)
  between operations  13.6 us (4%)
  matrix products  12.6 us (4%)
  local copies, waits for them, and re-layouts  9.98 us (3%)
  other arithmetic  6.47 us (2%)
    all_gather x1, waiting for transfers between devices, body(): piece = lax.all_gather(arrived, 'ep', axis=3, tiled=True)  82.4 us
    all_gather x1, waiting for transfers between devices, body(): lax.all_gather(hidden, 'ep', axis=3, tiled=True)  71.7 us
    all_to_all x1, blocking collectives, body(): lax.all_to_all(buffer, TP, split_axis=0, concat_axis=0, tiled=True)  47.4 us
    all_to_all x1, waiting for transfers between devices, turned_blocks(): lax.all_to_all(parts, axes[k], split_axis=k, concat_axis=k, tiled=True)  29.2 us
    all_to_all x1, starting transfers between devices, turned_blocks(): lax.all_to_all(parts, axes[k], split_axis=k, concat_axis=k, tiled=True)  12.7 us
    all_to_all x2, starting transfers between devices, sent_to_all(): return lax.all_to_all(copies, axis, split_axis=0, concat_axis=0, tiled=True)  12 us
    all_to_all x2, waiting for transfers between devices, sent_to_all(): return lax.all_to_all(copies, axis, split_axis=0, concat_axis=0, tiled=True)  10.8 us
  transfers between devices with their start and end apart: 5, of which 5 were waited for; matrix products, arithmetic and copies ran while one was open for 1% of the time, Pallas kernels for 0%

commit v1 on v0

--- a/solution.py
+++ b/solution.py
@@ -1,11 +1,24 @@
+import functools
 import jax
 import jax.numpy as jnp
 from jax import lax
 from jax.sharding import Mesh
 from jax.sharding import PartitionSpec as P
+from jax.lax import all_to_all, axis_size
 
 TP = ("tp_0", "tp_1")
 epsilon = 1e-06
+
+
+def _pass_pipes(my_tile, lane_axis):
+    formed = jnp.concatenate(
+        all_to_all(jnp.stack([my_tile for _ in range(axis_size(lane_axis))]), lane_axis, 0, 0),
+        axis=3,
+    )
+    return formed
+
+
+goods_read = functools.partial(_pass_pipes, lane_axis="ep")
 
 
 def sent_to_all(value, axis):
@@ -71,7 +84,7 @@
     )
     arrived = lax.all_to_all(buffer, TP, split_axis=0, concat_axis=0, tiled=True)
     arrived = arrived.reshape(n_route, local_experts, capacity, width_local)
-    piece = lax.all_gather(arrived, "ep", axis=3, tiled=True)
+    piece = goods_read(arrived)
     gate_sum = jnp.einsum("sect,eft->secf", piece, w_gate, preferred_element_type=jnp.float32)
     up_sum = jnp.einsum("sect,eft->secf", piece, w_up, preferred_element_type=jnp.float32)
     hidden = (jax.nn.silu(gate_sum) * up_sum).astype(jnp.bfloat16)

time: 314 us -> 353 us (1.12)
  blocking collectives: 51.6 us -> 151 us
  waiting for transfers between devices: 194 us -> 104 us
  local copies, waits for them, and re-layouts: 9.98 us -> 39.9 us
    all_to_all x0 -> x1, blocking collectives: none -> 99.6 us  [_pass_pipes(): all_to_all(jnp.stack([my_tile for _ in range(axis_size(lane_axis))]), lan...]
    all_gather x1 -> x0, waiting for transfers between devices: 82.4 us -> none  [body(): piece = lax.all_gather(arrived, 'ep', axis=3, tiled=True)]
    reshape x0 -> x1, local copies, waits for them, and re-layouts: none -> 15.1 us  [_pass_pipes(): jnp.concatenate(all_to_all(jnp.stack([my_tile for _ in range(axis_size(la...]
    another operation x1 -> x3, local copies, waits for them, and re-layouts: 0.01 us -> 14.6 us
    all_gather x1, waiting for transfers between devices: 71.7 us -> 63.9 us  [body(): lax.all_gather(hidden, 'ep', axis=3, tiled=True)]
  transfers between devices with their start and end apart: 5 -> 4, of which waited for: 5 -> 4; matrix products, arithmetic and copies ran while one was open for 1% -> 1% of each run, Pallas kernels for 0% -> 0%
where the time goes in v1:
time: 353 us; the launch traced here: 352 us
  blocking collectives  151 us (43%)
  waiting for transfers between devices  104 us (29%)
  local copies, waits for them, and re-layouts  39.9 us (11%)
  starting transfers between devices  24.7 us (7%)
  between operations  13.6 us (4%)
  matrix products  12.3 us (3%)
  other arithmetic  6.47 us (2%)
    all_to_all x1, blocking collectives, _pass_pipes(): all_to_all(jnp.stack([my_tile for _ in range(axis_size(lane_axis))]), lan...  99.6 us
    all_gather x1, waiting for transfers between devices, body(): lax.all_gather(hidden, 'ep', axis=3, tiled=True)  63.9 us
    all_to_all x1, blocking collectives, body(): lax.all_to_all(buffer, TP, split_axis=0, concat_axis=0, tiled=True)  47.3 us
    all_to_all x1, waiting for transfers between devices, turned_blocks(): lax.all_to_all(parts, axes[k], split_axis=k, concat_axis=k, tiled=True)  29.2 us
    reshape x1, local copies, waits for them, and re-layouts, _pass_pipes(): jnp.concatenate(all_to_all(jnp.stack([my_tile for _ in range(axis_size(la...  15.1 us
    another operation x2, local copies, waits for them, and re-layouts  13.6 us
    all_to_all x1, starting transfers between devices, turned_blocks(): lax.all_to_all(parts, axes[k], split_axis=k, concat_axis=k, tiled=True)  12.7 us
    all_to_all x2, starting transfers between devices, sent_to_all(): return lax.all_to_all(copies, axis, split_axis=0, concat_axis=0, tiled=True)  12 us
  transfers between devices with their start and end apart: 4, of which 4 were waited for; matrix products, arithmetic and copies ran while one was open for 1% of the time, Pallas kernels for 0%

profile of v1, /device:TPU:32, one launch (start us, length us, event | category | flops | bytes accessed | tf_op | source)
XLA Modules:
  0.0 351.9 jit_solution(9600843970639325818)
XLA Ops:
  6.5 1.1 fusion.10
  7.6 0.6 broadcast_in_dim.7
  8.3 7.0 %all-to-all-start = ((f32[16,1,256]{2,1,0:T(1,128)}), f32[16,1,256]{2,1,0:T(1,128)S(1)}, u32[]{:S(2)}, u32[]{:S(2)}) async-start(f32[16,1,256]{2,1,0:T(1,128)} %broadcast_in_dim.7), calls=%async_computation | async-start | bytes 32768 | tf_op jit(solution)/shard_map/all_to_all | solution.py:26
  15.4 0.8 copy.40
  16.5 0.7 broadcast_multiply_fusion
  17.2 1.2 reduce-window.6
  18.3 0.2 slice_reduce_fusion
  18.8 0.1 mul.74
  19.0 0.7 convert_element_type.44
  19.7 3.2 all-to-all-done
  22.9 1.0 fusion.12
  24.0 3.9 %scatter_custom_fusion = bf16[1024,256]{1,0:T(8,128)(2,1)S(1)} fusion(s32[512]{0:T(512)S(1)} %bitcast.71, bf16[256,256]{1,0:T(8,128)(2,1)S(1)} %fusion.12, s32[1024]{0:T(1024)S(1)} %pad_clamp_fusion.1, bf16[]{:T(256)} %constant.32.clone.1), kind=kCustom, calls=%fused_computation.19 | custom fusion | bytes 524290 | tf_op jit(solution)/shard_map/scatter | solution.py:83
  27.9 47.3 %all_to_all.36 = bf16[32,32,256]{2,1,0:T(8,128)(2,1)S(1)} all-to-all(bf16[32,32,256]{2,1,0:T(8,128)(2,1)S(1)} %bitcast.69), channel_id=1, replica_groups=mesh['ep'=16,'tp_0'=16,'tp_1'=2] {'tp_0','tp_1'}, dimensions={0} | all-to-all | bytes 1048576 | tf_op jit(solution)/shard_map/all_to_all | solution.py:85
  75.2 1.1 stack.3
  76.3 99.6 %all_to_all.37 = bf16[16,32,1,32,256]{4,3,1,2,0:T(8,128)(2,1)} all-to-all(bf16[16,32,1,32,256]{4,3,1,2,0:T(8,128)(2,1)S(1)} %stack.3), channel_id=1, replica_groups=mesh['ep'=16,'tp_0'=16,'tp_1'=2] {'ep'}, dimensions={0} | all-to-all | bytes 16777216 | tf_op jit(solution)/shard_map/all_to_all | solution.py:15
  175.9 15.1 %copy.44 = bf16[32,1,32,16,256]{4,3,2,0,1:T(8,128)(2,1)} copy(bf16[32,1,32,16,256]{4,2,0,1,3:T(8,128)(2,1)} %bitcast.67) | data formatting | bytes 16777216 | tf_op jit(solution)/shard_map/reshape | solution.py:14
  191.0 13.6 %reshape.149 = bf16[32,32,4096]{2,1,0:T(8,128)(2,1)} reshape(bf16[32,1,32,16,256]{4,3,2,0,1:T(8,128)(2,1)} %copy.44) | data formatting | bytes 16777216 | tf_op jit(solution)/shard_map/reshape.9
  204.6 5.9 %convolution_bitcast_fusion.1 = f32[32,1,32,128]{3,2,0,1:T(8,128)S(1)} fusion(bf16[32,32,4096]{2,1,0:T(8,128)(2,1)} %reshape.149, bf16[1,128,4096]{2,1,0:T(8,128)(2,1)S(1)} %copy-done.3), kind=kOutput, calls=%fused_computation.8 | convolution fusion | flops 1073741824 | bytes 9961472 | tf_op jit(solution)/shard_map/sect,eft->secf/dot_general | solution.py:88
  210.6 3.0 fusion.6
  213.7 63.9 %all-gather.2.cloned.1.call-done = bf16[32,1,32,2048]{3,2,0,1:T(8,128)(2,1)} async-done(((bf16[32,1,32,128]{3,2,0,1:T(8,128)(2,1)}), bf16[32,1,32,2048]{3,2,0,1:T(8,128)(2,1)}) %all-gather.2.cloned.1.call-update) | async-done | bytes 4194320 | tf_op jit(solution)/shard_map/all_gather | solution.py:93
  277.5 3.4 fusion.2
  281.0 4.2 %all_to_all.38 = bf16[16,2,32,256]{3,2,0,1:T(8,128)(2,1)S(1)} all-to-all(bf16[16,2,32,256]{3,2,0,1:T(8,128)(2,1)S(1)} %copy.45), channel_id=1, replica_groups=mesh['ep'=16,'tp_0'=16,'tp_1'=2] {'tp_1'}, dimensions={1} | all-to-all | bytes 1048576 | tf_op jit(solution)/shard_map/all_to_all | solution.py:49
  285.2 0.8 copy.46
  286.0 12.7 %all-to-all-start.4 = ((bf16[16,2,32,256]{3,2,1,0:T(8,128)(2,1)}), bf16[16,2,32,256]{3,2,1,0:T(8,128)(2,1)S(1)}, u32[]{:S(2)}, u32[]{:S(2)}) async-start(bf16[16,2,32,256]{3,2,1,0:T(8,128)(2,1)} %copy.46), calls=%async_computation.4 | async-start | bytes 1048576 | tf_op jit(solution)/shard_map/all_to_all | solution.py:49
  298.8 29.2 %all-to-all-done.4 = bf16[16,2,32,256]{3,2,1,0:T(8,128)(2,1)S(1)} async-done(((bf16[16,2,32,256]{3,2,1,0:T(8,128)(2,1)}), bf16[16,2,32,256]{3,2,1,0:T(8,128)(2,1)S(1)}, u32[]{:S(2)}, u32[]{:S(2)}) %all-to-all-start.4) | async-done | bytes 524320 | tf_op jit(solution)/shard_map/all_to_all | solution.py:49
  328.1 1.9 gather_fusion
  330.0 0.3 reshape.154
  330.3 0.7 multiply_reduce_fusion
  331.1 0.6 broadcast_in_dim.8
  331.7 4.9 %all-to-all-start.5 = ((f32[16,1,256]{2,1,0:T(1,128)}), f32[16,1,256]{2,1,0:T(1,128)S(1)}, u32[]{:S(2)}, u32[]{:S(2)}) async-start(f32[16,1,256]{2,1,0:T(1,128)} %broadcast_in_dim.8), calls=%async_computation.5 | async-start | bytes 32768 | tf_op jit(solution)/shard_map/all_to_all | solution.py:26
  336.7 7.6 %all-to-all-done.5 = f32[16,1,256]{2,1,0:T(1,128)S(1)} async-done(((f32[16,1,256]{2,1,0:T(1,128)}), f32[16,1,256]{2,1,0:T(1,128)S(1)}, u32[]{:S(2)}, u32[]{:S(2)}) %all-to-all-start.5) | async-done | bytes 16416 | tf_op jit(solution)/shard_map/all_to_all | solution.py:26
  344.3 0.8 multiply_convert_fusion
  (33 shorter events, 1.2 us)
Async XLA Ops:
  6.5 271.0 %copy-start = (bf16[1,2048,256]{2,1,0:T(8,128)(2,1)S(1)}, bf16[1,2048,256]{2,1,0:T(8,128)(2,1)}, u32[]{:S(2)}) copy-start(bf16[1,2048,256]{2,1,0:T(8,128)(2,1)} %param.14) | copy-start | bytes 3145732
  8.3 14.6 %all-to-all-start = ((f32[16,1,256]{2,1,0:T(1,128)}), f32[16,1,256]{2,1,0:T(1,128)S(1)}, u32[]{:S(2)}, u32[]{:S(2)}) async-start(f32[16,1,256]{2,1,0:T(1,128)} %broadcast_in_dim.7), calls=%async_computation | async-start | bytes 32768 | tf_op jit(solution)/shard_map/all_to_all | solution.py:26
  15.3 262.2 %all-gather.2.cloned.1.call-start = ((), (), s32[]{:S(2)}) async-start(), calls=%async_computation.6 | async-start | bytes 4456448 | tf_op jit(solution)/shard_map/all_gather | solution.py:93
  191.0 13.6 %copy-start.3 = (bf16[1,128,4096]{2,1,0:T(8,128)(2,1)S(1)}, bf16[1,128,4096]{2,1,0:T(8,128)(2,1)}, u32[]{:S(2)}) copy-start(bf16[1,128,4096]{2,1,0:T(8,128)(2,1)} %param.12) | copy-start | bytes 3145732
  204.6 5.9 %copy-start.1 = (bf16[32,32,4096]{2,1,0:T(8,128)(2,1)S(1)}, bf16[32,32,4096]{2,1,0:T(8,128)(2,1)}, u32[]{:S(2)}) copy-start(bf16[32,32,4096]{2,1,0:T(8,128)(2,1)} %reshape.149) | copy-start | bytes 25165828
  204.6 6.0 %copy-start.4 = (bf16[1,128,4096]{2,1,0:T(8,128)(2,1)S(1)}, bf16[1,128,4096]{2,1,0:T(8,128)(2,1)}, u32[]{:S(2)}) copy-start(bf16[1,128,4096]{2,1,0:T(8,128)(2,1)} %param.13) | copy-start | bytes 3145732
  213.6 85.0 %copy-start.2 = (f32[256,2]{0,1:T(2,128)S(1)}, f32[256,2]{0,1:T(2,128)}, u32[]{:S(2)}) copy-start(f32[256,2]{0,1:T(2,128)} %param.11) | copy-start | bytes 6148
  213.6 123.0 %copy-start.5 = (bf16[256]{0:T(256)(128)(2,1)S(1)}, bf16[256]{0:T(256)(128)(2,1)}, u32[]{:S(2)}) copy-start(bf16[256]{0:T(256)(128)(2,1)} %param.15) | copy-start | bytes 1540
  286.0 42.1 %all-to-all-start.4 = ((bf16[16,2,32,256]{3,2,1,0:T(8,128)(2,1)}), bf16[16,2,32,256]{3,2,1,0:T(8,128)(2,1)S(1)}, u32[]{:S(2)}, u32[]{:S(2)}) async-start(bf16[16,2,32,256]{3,2,1,0:T(8,128)(2,1)} %copy.46), calls=%async_computation.4 | async-start | bytes 1048576 | tf_op jit(solution)/shard_map/all_to_all | solution.py:49
  331.7 12.5 %all-to-all-start.5 = ((f32[16,1,256]{2,1,0:T(1,128)}), f32[16,1,256]{2,1,0:T(1,128)S(1)}, u32[]{:S(2)}, u32[]{:S(2)}) async-start(f32[16,1,256]{2,1,0:T(1,128)} %broadcast_in_dim.8), calls=%async_computation.5 | async-start | bytes 32768 | tf_op jit(solution)/shard_map/all_to_all | solution.py:26
Sparse Core Ops, SparseCore 0:
  213.8 63.7 all-gather.1
